TPU v7x, 512 devices: a 8x2x16 block of a 8x8x16 slice. The times are simulated.
512 devices in a mesh: grp: 2 (over y), sp: 32 (over z, core), tp: 8 (over x).
Axes of the slice: x: 8, y: 2, z: 16, core: 2. Of those that a mesh axis runs over, the one named last changes fastest.
The devices are a block of a 8x8x16 slice.
Arguments:
- tokens: bfloat16 [16384, 4096], P(('grp', 'sp')), parts along dimension 0, may hold values from -6 to 6
- norm_gain: bfloat16 [2, 4096], replicated, may hold values from 0.099609375 to 1.8984375
- w_query: bfloat16 [2, 4096, 2048], P(None, 'sp', 'tp'), may hold values from -0.09375 to 0.09375
- w_key: bfloat16 [2, 4096, 2048], P(None, 'sp', 'tp'), may hold values from -0.09375 to 0.09375
- w_value: bfloat16 [2, 4096, 2048], P(None, 'sp', 'tp'), may hold values from -0.09375 to 0.09375
- w_out: bfloat16 [2, 2048, 4096], P(None, 'tp', 'sp'), may hold values from -0.125 to 0.125
- offset_bias: float32 [2, 16, 15, 31], P(None, 'tp'), may hold values from -4 to 300
Outputs:
- mixed: bfloat16 [16384, 4096], P(('grp', 'sp')), parts along dimension 0
There are 2 independent parts, one for each index of `grp`. A program takes and returns all parts, laid end to end along the dimension named above; an argument that names none is the same for every part. Nothing has to cross between parts.
All inputs are finite; a program needn't handle non-finite values.
Results may differ from a plain program's by a relative error of at most 0.013.
Values may be sent and summed in bfloat16 or wider, within the bound.
A program may use at most 128 MiB of HBM per device.

v0:
```python
import jax
import jax.numpy as jnp
from jax import lax
from jax.sharding import PartitionSpec as P

HD = 128
GRID_W = 64
KR = 8
KC = 16
LAYERS = 2
norm_eps = 1e-06


def turned_gather(arrays, axis, dims):
    turned = [jnp.moveaxis(a, dim, 0) for a, dim in zip(arrays, dims)]
    both = jnp.concatenate([t.reshape(len(t), -1) for t in turned], axis=1)
    result, at, outs = (lax.all_gather(both, axis, axis=0, tiled=True), 0, [])
    for t, dim in zip(turned, dims):
        share = result[:, at : at + t[0].size].reshape(-1, *t.shape[1:])
        outs.append(jnp.moveaxis(share, 0, dim))
        at += t[0].size
    return tuple(outs)


def with_halo(block, sides, width):
    for axis, dim in sides:
        count = lax.axis_size(axis)
        forward = [(i, i + 1) for i in range(count - 1)]
        backward = [(target, source) for source, target in forward]
        low = lax.ppermute(
            lax.slice_in_dim(block, block.shape[dim] - width, None, axis=dim), axis, forward
        )
        high = lax.ppermute(lax.slice_in_dim(block, 0, width, axis=dim), axis, backward)
        block = jnp.concatenate([low, block, high], axis=dim)
    return block


def rms_rows(values, gain):
    wide = values.astype(jnp.float32)
    scaled = wide * lax.rsqrt(jnp.mean(wide * wide, axis=-1, keepdims=True) + norm_eps)
    return (scaled * gain.astype(jnp.float32)).astype(jnp.bfloat16)


def gather_rows(block_rows):
    return lax.all_gather(block_rows, "tp", axis=0, tiled=True)


def on_device(tokens, norm_gain, w_query, w_key, w_value, w_out, offset_bias):
    sp_count = lax.axis_size("sp")
    sp_index = lax.axis_index("sp")
    tp_count = lax.axis_size("tp")
    tp_index = lax.axis_index("tp")
    tok_rows = tokens.shape[0]
    local_rows = tok_rows // GRID_W
    grid_rows = local_rows * sp_count
    heads_here = offset_bias.shape[1]
    head_width = heads_here * HD
    share_rows = tok_rows // tp_count
    reach = KR // 2
    scale = HD ** (-0.5)
    columns = jnp.arange(GRID_W, dtype=jnp.int32)
    col_first = jnp.clip(columns - KC // 2, 0, GRID_W - KC)
    col_inside = (columns[None, :] >= col_first[:, None]) & (
        columns[None, :] < col_first[:, None] + KC
    )
    col_offset = jnp.clip(columns[None, :] - columns[:, None], 1 - KC, KC - 1) + KC - 1
    col_onehot = (
        jnp.arange(2 * KC - 1, dtype=jnp.int32)[:, None, None] == col_offset[None, :, :]
    ).astype(jnp.float32)
    first_row = sp_index * local_rows
    own_rows = first_row + jnp.arange(local_rows, dtype=jnp.int32)
    row_first = jnp.clip(own_rows - reach, 0, grid_rows - KR)
    band_start = row_first - first_row + reach
    row_offset = (
        row_first[:, None] + jnp.arange(KR, dtype=jnp.int32)[None, :] - own_rows[:, None] + KR - 1
    )
    row_onehot = (
        row_offset[:, :, None] == jnp.arange(2 * KR - 1, dtype=jnp.int32)[None, None, :]
    ).astype(jnp.float32)
    every_query, every_key, every_value, every_out = turned_gather(
        (w_query, w_key, w_value, w_out), "sp", (1, 1, 1, 2)
    )
    residual = tokens
    for layer_index in range(LAYERS):
        if layer_index > 0:
            normed = gather_rows(rms_rows(residual, norm_gain[layer_index]))
        else:
            normed = rms_rows(residual, norm_gain[layer_index])
        queries = jnp.dot(normed, every_query[layer_index], preferred_element_type=jnp.float32)
        keys = jnp.dot(normed, every_key[layer_index], preferred_element_type=jnp.float32)
        values = jnp.dot(normed, every_value[layer_index], preferred_element_type=jnp.float32)
        out_weight = every_out[layer_index]
        queries = queries.astype(jnp.bfloat16).reshape(local_rows, GRID_W, heads_here, HD)
        key_values = jnp.concatenate(
            [keys.astype(jnp.bfloat16), values.astype(jnp.bfloat16)], axis=1
        )
        key_values = key_values.reshape(local_rows, GRID_W, 2 * head_width)
        padded = with_halo(key_values, (("sp", 0),), reach)
        bands = jax.vmap(lambda band_begin: lax.dynamic_slice_in_dim(padded, band_begin, KR, 0))(
            band_start
        )
        band_keys = bands[..., :head_width].reshape(local_rows, KR, GRID_W, heads_here, HD)
        band_values = bands[..., head_width:].reshape(local_rows, KR, GRID_W, heads_here, HD)
        col_bias = jnp.einsum(
            "hro,oqk->hrqk", offset_bias[layer_index], col_onehot, precision=lax.Precision.HIGHEST
        )
        full_bias = jnp.einsum(
            "ijr,hrqk->hiqjk", row_onehot, col_bias, precision=lax.Precision.HIGHEST
        )
        scores = jnp.einsum(
            "iqhd,ijkhd->hiqjk", queries, band_keys, preferred_element_type=jnp.float32
        )
        scores = scores * scale + full_bias
        scores = jnp.where(col_inside[None, None, :, None, :], scores, -jnp.inf)
        flattened = scores.reshape(heads_here, local_rows, GRID_W, KR * GRID_W)
        weights = jax.nn.softmax(flattened, axis=-1).astype(jnp.bfloat16)
        weights = weights.reshape(heads_here, local_rows, GRID_W, KR, GRID_W)
        attended = jnp.einsum(
            "hiqjk,ijkhd->iqhd", weights, band_values, preferred_element_type=jnp.float32
        )
        attended = attended.astype(jnp.bfloat16).reshape(tok_rows, head_width)

        def term_rows(row_begin, row_count, attended=attended, out_weight=out_weight):
            return jnp.dot(attended, out_weight, preferred_element_type=jnp.float32)

        branch = lax.psum_scatter(
            term_rows(jnp.int32(0), lax.axis_size("tp") * share_rows).astype(jnp.bfloat16),
            "tp",
            scatter_dimension=0,
            tiled=True,
        ).astype(jnp.float32)
        if layer_index > 0:
            own_part = residual
        else:
            own_part = lax.dynamic_slice_in_dim(tokens, tp_index * share_rows, share_rows, 0)
        residual = (own_part.astype(jnp.float32) + branch).astype(jnp.bfloat16)
    residual = gather_rows(residual)
    return residual


def solution(mesh):
    return jax.shard_map(
        on_device,
        mesh=mesh,
        in_specs=(
            P(("grp", "sp"), None),
            P(),
            P(None, "sp", "tp"),
            P(None, "sp", "tp"),
            P(None, "sp", "tp"),
            P(None, "tp", "sp"),
            P(None, "tp", None, None),
        ),
        out_specs=P(("grp", "sp"), None),
        check_vma=False,
    )
```

profile of v0, /device:TPU:66, one launch (start us, length us, event | category | flops | bytes accessed | tf_op | source)
XLA Modules:
  0.0 439.5 jit_solution(5943801142886471088)
XLA Ops:
  6.6 1.0 copy.20
  7.6 1.0 copy.21
  8.6 1.0 copy.22
  9.7 1.7 pad_maximum_fusion.2
  11.7 0.7 convolution_bitcast_fusion.1
  12.5 2.4 fusion.52
  14.9 2.3 copy.26
  17.2 0.6 shift-left_bitcast_fusion
  17.8 2.1 fusion
  19.9 0.6 slice_convert_fusion
  20.6 156.0 %all-gather.4.cloned.1.call-done = bf16[4096,2048]{0,1:T(8,128)(2,1)} async-done(((bf16[128,2048]{0,1:T(8,128)(2,1)}), bf16[4096,2048]{0,1:T(8,128)(2,1)}) %all-gather.4.cloned.1.call-update) | async-done | bytes 16777232 | tf_op jit(solution)/shard_map/all_gather | solution.py:17
  176.6 10.2 %fusion.60 = (bf16[4096,512]{0,1:T(8,128)(2,1)}, bf16[4096,512]{0,1:T(8,128)(2,1)}, bf16[4096,512]{0,1:T(8,128)(2,1)S(1)}, bf16[4096,512]{0,1:T(8,128)(2,1)S(1)}) fusion(bf16[4096,2048]{0,1:T(8,128)(2,1)} %all-gather.4.cloned.1.call-done), kind=kLoop, calls=%fused_computation.110 | loop fusion | bytes 33554432 | tf_op jit(solution)/shard_map/slice | solution.py:19
  186.8 1.0 fusion.15
  187.7 1.0 copy-done.2
  188.7 1.0 fusion.16
  190.1 2.2 collective-permute-start
  192.3 1.3 collective-permute-start.1
  193.7 3.0 fusion.17
  196.7 0.7 copy-done.7
  197.4 1.1 pad_maximum_fusion
  198.6 2.1 gather_fusion
  200.7 1.9 slice_bitcast_fusion.30
  202.6 0.6 fusion.61
  204.2 1.5 copy-done
  205.7 2.0 convolution_convert_fusion.1
  207.9 48.9 %reduce-scatter.3.cloned.1.call-done = bf16[32,4096]{1,0:T(8,128)(2,1)} async-done(((bf16[256,4096]{1,0:T(8,128)(2,1)}), bf16[32,4096]{1,0:T(8,128)(2,1)}) %reduce-scatter.3.cloned.1.call-update) | async-done | bytes 262160 | tf_op jit(solution)/shard_map/reduce_scatter | solution.py:126
  256.9 1.2 fusion.36
  258.1 0.8 fusion.38
  259.3 0.7 convolution_bitcast_fusion
  260.0 2.3 fusion.50
  262.3 2.3 copy.33
  264.7 41.1 %all-gather.6.cloned.1.call-done = bf16[256,4096]{1,0:T(8,128)(2,1)} async-done(((bf16[32,4096]{1,0:T(8,128)(2,1)}), bf16[256,4096]{1,0:T(8,128)(2,1)}) %all-gather.6.cloned.1.call-update) | async-done | bytes 2097168 | tf_op jit(solution)/shard_map/all_gather | solution.py:45
  305.8 3.1 fusion.18
  309.2 2.3 fusion.19
  311.8 1.3 collective-permute-start.2
  313.1 1.3 collective-permute-start.3
  314.4 3.0 fusion.20
  317.4 0.7 copy-done.8
  318.6 1.2 pad_maximum_fusion.1
  319.8 2.0 gather_fusion.1
  321.8 1.9 slice_bitcast_fusion.28
  323.7 0.6 fusion.62
  325.3 1.5 copy-done.1
  326.8 2.0 convolution_convert_fusion
  329.0 52.1 %reduce-scatter.5.cloned.1.call-done = bf16[32,4096]{1,0:T(8,128)(2,1)} async-done(((bf16[256,4096]{1,0:T(8,128)(2,1)}), bf16[32,4096]{1,0:T(8,128)(2,1)}) %reduce-scatter.5.cloned.1.call-update) | async-done | bytes 262160 | tf_op jit(solution)/shard_map/reduce_scatter | solution.py:126
  381.1 1.7 fusion.39
  382.9 46.9 %all-gather.8.cloned.1.call-done = bf16[256,4096]{1,0:T(8,128)(2,1)} async-done(((bf16[32,4096]{1,0:T(8,128)(2,1)}), bf16[256,4096]{1,0:T(8,128)(2,1)}) %all-gather.8.cloned.1.call-update) | async-done | bytes 2097168 | tf_op jit(solution)/shard_map/all_gather | solution.py:45
  429.8 3.1 copy.111
  (60 shorter events, 4.5 us)
Async XLA Ops:
  6.5 5.0 %copy-start.12 = (f32[2,2,15,31]{3,1,2,0:T(2,128)S(1)}, f32[2,2,15,31]{3,1,2,0:T(2,128)}, u32[]{:S(2)}) copy-start(f32[2,2,15,31]{3,1,2,0:T(2,128)} %param.13) | copy-start | bytes 22324
  6.5 170.0 %all-gather.4.cloned.1.call-start = ((), (), s32[]{:S(2)}) async-start(), calls=%async_computation.2 | async-start | bytes 17301504 | tf_op jit(solution)/shard_map/all_gather | solution.py:17
  11.5 245.4 %reduce-scatter.3.cloned.1.call-start = ((), (), s32[]{:S(2)}) async-start(), calls=%async_computation.3 | async-start | bytes 2359296 | tf_op jit(solution)/shard_map/reduce_scatter | solution.py:126
  12.5 2.4 copy-start.13
  17.2 2.7 copy-start.9
  176.6 10.2 %copy-start.5 = (bf16[256,4096]{1,0:T(8,128)(2,1)S(1)}, bf16[256,4096]{1,0:T(8,128)(2,1)}, u32[]{:S(2)}) copy-start(bf16[256,4096]{1,0:T(8,128)(2,1)} %param.7) | copy-start | bytes 6291460
  186.7 1.9 copy-start.2
  186.7 3.2 copy-start.4
  190.1 6.6 %collective-permute-start = (bf16[4,64,512]{2,1,0:T(8,128)(2,1)S(1)}, bf16[4,64,512]{2,1,0:T(8,128)(2,1)S(1)}, u32[]{:S(2)}, u32[]{:S(2)}) collective-permute-start(bf16[4,64,512]{2,1,0:T(8,128)(2,1)S(1)} %bitcast.167), channel_id=1, source_target_pairs={{0,8},{8,16},{16,24},{24,32},{32,40},{40,48},{48,56},{56,64},{64,7... | collective-permute-start | bytes 786440 | tf_op jit(solution)/shard_map/ppermute | solution.py:30
  192.3 5.1 %collective-permute-start.1 = (bf16[4,64,512]{2,1,0:T(8,128)(2,1)S(1)}, bf16[4,64,512]{2,1,0:T(8,128)(2,1)}, u32[]{:S(2)}, u32[]{:S(2)}) collective-permute-start(bf16[4,64,512]{2,1,0:T(8,128)(2,1)S(1)} %bitcast.168), channel_id=1, source_target_pairs={{8,0},{16,8},{24,16},{32,24},{40,32},{48,40},{56,48},{64,56},{72,6... | collective-permute-start | bytes 786440 | tf_op jit(solution)/shard_map/ppermute | solution.py:33
  196.7 0.7 copy-start.7
  203.6 2.2 copy-start
  207.8 50.3 %copy-start.10 = (f32[1,4096]{1,0:T(1,128)S(1)}, f32[1,4096]{1,0:T(1,128)}, u32[]{:S(2)}) copy-start(f32[1,4096]{1,0:T(1,128)} %get-tuple-element.17) | copy-start | bytes 49156
  207.8 52.2 %copy-start.14 = (s32[4,8]{1,0:T(4,128)S(1)}, s32[4,8]{1,0:T(4,128)}, u32[]{:S(2)}) copy-start(s32[4,8]{1,0:T(4,128)} %copy-done.13) | copy-start | bytes 388
  207.8 97.9 %all-gather.6.cloned.1.call-start = ((), (), s32[]{:S(2)}) async-start(), calls=%async_computation.4 | async-start | bytes 2359296 | tf_op jit(solution)/shard_map/all_gather | solution.py:45
  259.0 122.1 %reduce-scatter.5.cloned.1.call-start = ((), (), s32[]{:S(2)}) async-start(), calls=%async_computation.5 | async-start | bytes 2359296 | tf_op jit(solution)/shard_map/reduce_scatter | solution.py:126
  305.8 3.4 copy-start.3
  311.7 5.6 %copy-start.6 = (bf16[256,512]{1,0:T(8,128)(2,1)}, bf16[256,512]{1,0:T(8,128)(2,1)S(1)}, u32[]{:S(2)}) copy-start(bf16[256,512]{1,0:T(8,128)(2,1)S(1)} %copy.30) | copy-start | bytes 786436
  311.8 8.0 %copy-start.11 = (s32[4]{0:T(128)S(1)}, s32[4]{0:T(128)}, u32[]{:S(2)}) copy-start(s32[4]{0:T(128)} %shift-left_bitcast_fusion) | copy-start | bytes 52
  311.8 5.7 %collective-permute-start.2 = (bf16[4,64,512]{2,1,0:T(8,128)(2,1)S(1)}, bf16[4,64,512]{2,1,0:T(8,128)(2,1)S(1)}, u32[]{:S(2)}, u32[]{:S(2)}) collective-permute-start(bf16[4,64,512]{2,1,0:T(8,128)(2,1)S(1)} %bitcast.170), channel_id=1, source_target_pairs={{0,8},{8,16},{16,24},{24,32},{32,40},{40,48},{48,56},{56,64},{64,7... | collective-permute-start | bytes 786440 | tf_op jit(solution)/shard_map/ppermute | solution.py:30
  313.1 5.5 %collective-permute-start.3 = (bf16[4,64,512]{2,1,0:T(8,128)(2,1)S(1)}, bf16[4,64,512]{2,1,0:T(8,128)(2,1)}, u32[]{:S(2)}, u32[]{:S(2)}) collective-permute-start(bf16[4,64,512]{2,1,0:T(8,128)(2,1)S(1)} %bitcast.171), channel_id=1, source_target_pairs={{8,0},{16,8},{24,16},{32,24},{40,32},{48,40},{56,48},{64,56},{72,6... | collective-permute-start | bytes 786440 | tf_op jit(solution)/shard_map/ppermute | solution.py:33
  317.4 0.7 copy-start.8
  324.6 2.2 copy-start.1
  328.9 100.9 %all-gather.8.cloned.1.call-start = ((), (), s32[]{:S(2)}) async-start(), calls=%async_computation.6 | async-start | bytes 2359296 | tf_op jit(solution)/shard_map/all_gather | solution.py:45
Sparse Core Ops, SparseCore 0:
  11.6 164.9 all-gather.3
  208.0 48.8 reduce-scatter.2
  259.1 46.6 all-gather.5
  329.0 52.0 reduce-scatter.4
  383.1 46.6 all-gather.7
where the time goes:
time: 440 us; the launch traced here: 439 us
  waiting for transfers between devices  346 us (79%)
  local copies, waits for them, and re-layouts  35.7 us (8%)
  matrix products  25.7 us (6%)
  between operations  13.6 us (3%)
  other arithmetic  12.2 us (3%)
  starting transfers between devices  6.58 us (1%)
    all_gather x1, waiting for transfers between devices, turned_gather(): result, at, outs = (lax.all_gather(both, axis, axis=0, tiled=True), 0, [])  156 us
    reduce_scatter x2, waiting for transfers between devices, on_device(): lax.psum_scatter(term_rows(jnp.int32(0), lax.axis_size('tp') * share_rows...  101 us
    all_gather x2, waiting for transfers between devices, gather_rows(): return lax.all_gather(block_rows, 'tp', axis=0, tiled=True)  88 us
    unnamed x36, local copies, waits for them, and re-layouts  16.1 us
    slice x1, local copies, waits for them, and re-layouts, turned_gather(): share = result[:, at:at + t[0].size].reshape(-1, *t.shape[1:])  10.2 us
  transfers between devices with their start and end apart: 9, of which 6 were waited for; matrix products, arithmetic and copies ran while one was open for 5% of the time, Pallas kernels for 0%

commit v1 on v0

--- a/solution.py
+++ b/solution.py
@@ -9,6 +9,11 @@
 KC = 16
 LAYERS = 2
 norm_eps = 1e-06
+
+
+def gather_by_exchange(array, axis, dim):
+    copies = jnp.concatenate([array] * lax.axis_size(axis), axis=dim)
+    return lax.all_to_all(copies, axis, dim, dim, tiled=True)
 
 
 def turned_gather(arrays, axis, dims):
@@ -42,7 +47,7 @@
 
 
 def gather_rows(block_rows):
-    return lax.all_gather(block_rows, "tp", axis=0, tiled=True)
+    return gather_by_exchange(block_rows, "tp", 0)
 
 
 def on_device(tokens, norm_gain, w_query, w_key, w_value, w_out, offset_bias):

time: 440 us -> 451 us (1.025)
  blocking collectives: 0 us -> 51.3 us
  waiting for transfers between devices: 346 us -> 297 us
  starting transfers between devices: 6.58 us -> 11.8 us
    all_gather x2 -> x0, waiting for transfers between devices: 88 us -> none  [gather_rows(): return lax.all_gather(block_rows, 'tp', axis=0, tiled=True)]
    all_to_all x0 -> x1, blocking collectives: none -> 51.3 us  [gather_by_exchange(): return lax.all_to_all(copies, axis, dim, dim, tiled=True)]
    all_to_all x0 -> x1, waiting for transfers between devices: none -> 40.8 us  [gather_by_exchange(): return lax.all_to_all(copies, axis, dim, dim, tiled=True)]
    unnamed x0 -> x8, other arithmetic: none -> 6.84 us
    all_to_all x0 -> x1, starting transfers between devices: none -> 5.57 us  [gather_by_exchange(): return lax.all_to_all(copies, axis, dim, dim, tiled=True)]
    unnamed x36 -> x40, local copies, waits for them, and re-layouts: 16.1 us -> 15 us
  transfers between devices with their start and end apart: 9 -> 8, of which waited for: 6 -> 5; matrix products, arithmetic and copies ran while one was open for 5% -> 5% of each run, Pallas kernels for 0% -> 0%
where the time goes in v1:
time: 451 us
  waiting for transfers between devices  297 us (66%)
  blocking collectives  51.3 us (11%)
  local copies, waits for them, and re-layouts  35.2 us (8%)
  matrix products  25.7 us (6%)
  other arithmetic  16.5 us (4%)
  between operations  13.6 us (3%)
  starting transfers between devices  11.8 us (3%)
    all_gather x1, waiting for transfers between devices, turned_gather(): result, at, outs = (lax.all_gather(both, axis, axis=0, tiled=True), 0, [])  155 us
    reduce_scatter x2, waiting for transfers between devices, on_device(): lax.psum_scatter(term_rows(jnp.int32(0), lax.axis_size('tp') * share_rows...  99.9 us
    all_to_all x1, blocking collectives, gather_by_exchange(): return lax.all_to_all(copies, axis, dim, dim, tiled=True)  51.3 us
    all_to_all x1, waiting for transfers between devices, gather_by_exchange(): return lax.all_to_all(copies, axis, dim, dim, tiled=True)  40.8 us
    unnamed x40, local copies, waits for them, and re-layouts  15 us
    slice x1, local copies, waits for them, and re-layouts, turned_gather(): share = result[:, at:at + t[0].size].reshape(-1, *t.shape[1:])  10.2 us
  transfers between devices with their start and end apart: 8, of which 5 were waited for; matrix products, arithmetic and copies ran while one was open for 5% of the time, Pallas kernels for 0%

profile of v1, /device:TPU:66, one launch (start us, length us, event | category | flops | bytes accessed | tf_op | source)
XLA Modules:
  0.0 450.7 jit_solution(13433619927641621776)
XLA Ops:
  6.6 1.0 copy.20
  7.6 1.0 copy.21
  8.6 1.0 copy.22
  9.7 1.7 pad_maximum_fusion.2
  13.7 2.3 fusion.52
  16.0 2.3 copy.26
  18.9 2.1 fusion
  21.1 155.5 %all-gather.2.cloned.1.call-done = bf16[4096,2048]{0,1:T(8,128)(2,1)} async-done(((bf16[128,2048]{0,1:T(8,128)(2,1)}), bf16[4096,2048]{0,1:T(8,128)(2,1)}) %all-gather.2.cloned.1.call-update) | async-done | bytes 16777232 | tf_op jit(solution)/shard_map/all_gather | solution.py:22
  176.6 10.2 %fusion.61 = (bf16[4096,512]{0,1:T(8,128)(2,1)}, bf16[4096,512]{0,1:T(8,128)(2,1)}, bf16[4096,512]{0,1:T(8,128)(2,1)S(1)}, bf16[4096,512]{0,1:T(8,128)(2,1)S(1)}) fusion(bf16[4096,2048]{0,1:T(8,128)(2,1)} %all-gather.2.cloned.1.call-done), kind=kLoop, calls=%fused_computation.126 | loop fusion | bytes 33554432 | tf_op jit(solution)/shard_map/slice | solution.py:24
  186.7 1.0 fusion.15
  187.7 1.0 copy-done.2
  188.7 1.0 fusion.16
  190.1 2.2 collective-permute-start
  192.3 1.3 collective-permute-start.1
  193.6 3.0 fusion.17
  197.4 1.1 pad_maximum_fusion
  198.5 2.1 gather_fusion
  200.7 1.9 slice_bitcast_fusion.30
  204.2 1.5 copy-done
  205.7 2.0 convolution_convert_fusion.1
  207.8 49.0 %reduce-scatter.3.cloned.1.call-done = bf16[32,4096]{1,0:T(8,128)(2,1)} async-done(((bf16[256,4096]{1,0:T(8,128)(2,1)}), bf16[32,4096]{1,0:T(8,128)(2,1)}) %reduce-scatter.3.cloned.1.call-update) | async-done | bytes 262160 | tf_op jit(solution)/shard_map/reduce_scatter | solution.py:131
  256.9 1.2 fusion.36
  258.1 0.8 constant_dynamic-update-slice_fusion.7
  259.0 0.8 constant_dynamic-update-slice_fusion.6
  259.8 0.8 constant_dynamic-update-slice_fusion.5
  260.6 0.8 constant_dynamic-update-slice_fusion.4
  261.4 0.8 constant_dynamic-update-slice_fusion.3
  262.3 0.8 constant_dynamic-update-slice_fusion.2
  263.1 0.8 constant_dynamic-update-slice_fusion.1
  263.9 0.8 constant_dynamic-update-slice_fusion
  264.8 5.6 %all-to-all-start = ((bf16[8,32,4096]{2,1,0:T(8,128)(2,1)}), bf16[8,32,4096]{2,1,0:T(8,128)(2,1)}, u32[]{:S(2)}, u32[]{:S(2)}) async-start(bf16[8,32,4096]{2,1,0:T(8,128)(2,1)} %bitcast.37), calls=%async_computation.1 | async-start | bytes 4194304 | tf_op jit(solution)/shard_map/all_to_all | solution.py:16
  271.1 2.4 fusion.50
  273.4 2.3 copy.33
  275.8 40.8 %all-to-all-done = bf16[8,32,4096]{2,1,0:T(8,128)(2,1)} async-done(((bf16[8,32,4096]{2,1,0:T(8,128)(2,1)}), bf16[8,32,4096]{2,1,0:T(8,128)(2,1)}, u32[]{:S(2)}, u32[]{:S(2)}) %all-to-all-start) | async-done | bytes 2097184 | tf_op jit(solution)/shard_map/all_to_all | solution.py:16
  316.6 3.1 fusion.18
  320.0 2.3 fusion.19
  322.5 1.3 collective-permute-start.2
  323.9 1.3 collective-permute-start.3
  325.2 3.0 fusion.20
  329.2 1.1 pad_maximum_fusion.1
  330.4 2.0 gather_fusion.1
  332.4 1.9 slice_bitcast_fusion.28
  335.9 1.5 copy-done.1
  337.4 2.0 convolution_convert_fusion
  339.5 50.8 %reduce-scatter.5.cloned.1.call-done = bf16[32,4096]{1,0:T(8,128)(2,1)} async-done(((bf16[256,4096]{1,0:T(8,128)(2,1)}), bf16[32,4096]{1,0:T(8,128)(2,1)}) %reduce-scatter.5.cloned.1.call-update) | async-done | bytes 262160 | tf_op jit(solution)/shard_map/reduce_scatter | solution.py:131
  390.4 1.0 constant_dynamic-update-slice_fusion.15
  391.6 51.3 %all_to_all.24 = bf16[8,32,4096]{2,1,0:T(8,128)(2,1)S(1)} all-to-all(bf16[8,32,4096]{2,1,0:T(8,128)(2,1)S(1)} %bitcast.172), channel_id=1, replica_groups=mesh['grp'=2,'sp'=32,'tp'=8] {'tp'}, dimensions={0} | all-to-all | bytes 4194304 | tf_op jit(solution)/shard_map/all_to_all | solution.py:16
  442.9 1.3 copy.125
  (69 shorter events, 9.8 us)
Async XLA Ops:
  6.5 5.0 %copy-start.11 = (f32[2,2,15,31]{3,1,2,0:T(2,128)S(1)}, f32[2,2,15,31]{3,1,2,0:T(2,128)}, u32[]{:S(2)}) copy-start(f32[2,2,15,31]{3,1,2,0:T(2,128)} %param.13) | copy-start | bytes 22324
  6.5 170.0 %all-gather.2.cloned.1.call-start = ((), (), s32[]{:S(2)}) async-start(), calls=%async_computation.4 | async-start | bytes 17301504 | tf_op jit(solution)/shard_map/all_gather | solution.py:22
  11.5 245.4 %reduce-scatter.3.cloned.1.call-start = ((), (), s32[]{:S(2)}) async-start(), calls=%async_computation.5 | async-start | bytes 2359296 | tf_op jit(solution)/shard_map/reduce_scatter | solution.py:131
  13.1 0.6 copy-start.12
  18.4 2.7 copy-start.9
  176.6 10.2 %copy-start.5 = (bf16[256,4096]{1,0:T(8,128)(2,1)S(1)}, bf16[256,4096]{1,0:T(8,128)(2,1)}, u32[]{:S(2)}) copy-start(bf16[256,4096]{1,0:T(8,128)(2,1)} %param.7) | copy-start | bytes 6291460
  186.7 2.0 copy-start.2
  186.7 3.2 copy-start.4
  190.1 6.6 %collective-permute-start = (bf16[4,64,512]{2,1,0:T(8,128)(2,1)S(1)}, bf16[4,64,512]{2,1,0:T(8,128)(2,1)S(1)}, u32[]{:S(2)}, u32[]{:S(2)}) collective-permute-start(bf16[4,64,512]{2,1,0:T(8,128)(2,1)S(1)} %bitcast.181), channel_id=1, source_target_pairs={{0,8},{8,16},{16,24},{24,32},{32,40},{40,48},{48,56},{56,64},{64,7... | collective-permute-start | bytes 786440 | tf_op jit(solution)/shard_map/ppermute | solution.py:35
  192.3 5.1 %collective-permute-start.1 = (bf16[4,64,512]{2,1,0:T(8,128)(2,1)S(1)}, bf16[4,64,512]{2,1,0:T(8,128)(2,1)}, u32[]{:S(2)}, u32[]{:S(2)}) collective-permute-start(bf16[4,64,512]{2,1,0:T(8,128)(2,1)S(1)} %bitcast.182), channel_id=1, source_target_pairs={{8,0},{16,8},{24,16},{32,24},{40,32},{48,40},{56,48},{64,56},{72,6... | collective-permute-start | bytes 786440 | tf_op jit(solution)/shard_map/ppermute | solution.py:38
  196.7 0.7 copy-start.6
  203.5 2.2 copy-start
  264.8 5.6 %copy-start.8 = (f32[2,15,31,1]{2,0,1,3:T(2,128)S(1)}, f32[2,15,31,1]{2,0,1,3:T(2,128)}, u32[]{:S(2)}) copy-start(f32[2,15,31,1]{2,0,1,3:T(2,128)} %get-tuple-element.17) | copy-start | bytes 11164
  264.8 6.3 %copy-start.13 = (s32[4,8]{1,0:T(4,128)S(1)}, s32[4,8]{1,0:T(4,128)}, u32[]{:S(2)}) copy-start(s32[4,8]{1,0:T(4,128)} %copy-done.12) | copy-start | bytes 388
  264.8 51.8 %all-to-all-start = ((bf16[8,32,4096]{2,1,0:T(8,128)(2,1)}), bf16[8,32,4096]{2,1,0:T(8,128)(2,1)}, u32[]{:S(2)}, u32[]{:S(2)}) async-start(bf16[8,32,4096]{2,1,0:T(8,128)(2,1)} %bitcast.37), calls=%async_computation.1 | async-start | bytes 4194304 | tf_op jit(solution)/shard_map/all_to_all | solution.py:16
  270.3 120.0 %reduce-scatter.5.cloned.1.call-start = ((), (), s32[]{:S(2)}) async-start(), calls=%async_computation.6 | async-start | bytes 2359296 | tf_op jit(solution)/shard_map/reduce_scatter | solution.py:131
  316.6 3.4 copy-start.3
  322.5 7.8 %copy-start.10 = (s32[4]{0:T(128)S(1)}, s32[4]{0:T(128)}, u32[]{:S(2)}) copy-start(s32[4]{0:T(128)} %shift-left_bitcast_fusion) | copy-start | bytes 52
  322.5 5.7 %collective-permute-start.2 = (bf16[4,64,512]{2,1,0:T(8,128)(2,1)S(1)}, bf16[4,64,512]{2,1,0:T(8,128)(2,1)S(1)}, u32[]{:S(2)}, u32[]{:S(2)}) collective-permute-start(bf16[4,64,512]{2,1,0:T(8,128)(2,1)S(1)} %bitcast.184), channel_id=1, source_target_pairs={{0,8},{8,16},{16,24},{24,32},{32,40},{40,48},{48,56},{56,64},{64,7... | collective-permute-start | bytes 786440 | tf_op jit(solution)/shard_map/ppermute | solution.py:35
  323.9 5.4 %collective-permute-start.3 = (bf16[4,64,512]{2,1,0:T(8,128)(2,1)S(1)}, bf16[4,64,512]{2,1,0:T(8,128)(2,1)}, u32[]{:S(2)}, u32[]{:S(2)}) collective-permute-start(bf16[4,64,512]{2,1,0:T(8,128)(2,1)S(1)} %bitcast.185), channel_id=1, source_target_pairs={{8,0},{16,8},{24,16},{32,24},{40,32},{48,40},{56,48},{64,56},{72,6... | collective-permute-start | bytes 786440 | tf_op jit(solution)/shard_map/ppermute | solution.py:38
  328.2 0.7 copy-start.7
  335.2 2.2 copy-start.1
Sparse Core Ops, SparseCore 0:
  11.6 164.9 all-gather.1
  207.9 48.8 reduce-scatter.2
  339.7 50.6 reduce-scatter.4
